TPU v7x, 32 devices: a whole 2x2x4 slice. The times are simulated.
32 devices in a mesh: sp: 8 (over z, y), tp: 4 (over x, core).
Axes of the slice: x: 2, y: 2, z: 4, core: 2. Of those that a mesh axis runs over, the one named last changes fastest.
Arguments:
- stream: bfloat16 [2048, 2048], P('sp', 'tp'), may hold values from -6 to 6
- norm_gain: float32 [2, 2048], replicated, may hold values from 0.1 to 1.9
- w_value: bfloat16 [2, 2048, 1024], P(None, 'sp', 'tp'), may hold values from -0.125 to 0.125
- w_gate: bfloat16 [2, 2048, 1024], P(None, 'sp', 'tp'), may hold values from -0.125 to 0.125
- conv_taps: float32 [2, 128, 1024], P(None, None, 'tp'), as said below
- channel_gain: float32 [2, 1024], P(None, 'tp'), may hold values from 0.1 to 1.9
- w_out: bfloat16 [2, 1024, 2048], P(None, 'tp', 'sp'), may hold values from -0.1875 to 0.1875
Outputs:
- result: bfloat16 [2048, 2048], P('sp', 'tp')
Inputs may be any that keep to these rules, and one draw needn't show every extreme that they name: `conv_taps`: taps of each block of 128 consecutive channels share a scale factor of its own.
All inputs are finite; a program needn't handle non-finite values.
Results may differ from a plain program's by a relative error of at most 0.012.
Values may be sent and summed in bfloat16 or wider, within the bound.
A program may use at most 64 MiB of HBM per device.

v0:
```python
import jax
import jax.numpy as jnp
from jax import lax
from jax.sharding import PartitionSpec as P

C = 1024
LAYERS = 2


def from_behind(value, axis, steps):
    count = lax.axis_size(axis)
    initial, last = (max(0, -steps), min(count, count - steps))
    return lax.ppermute(value, axis, [(source, source + steps) for source in range(initial, last)])


def shards(stream, norm_gain, w_value, w_gate, conv_taps, channel_gain, w_out):
    x = stream
    tokens_here = stream.shape[0]
    local_ch = w_value.shape[2]
    taps = conv_taps.shape[1]
    for layer in range(LAYERS):
        whole = lax.all_gather(x, "tp", axis=1, tiled=True).astype(jnp.float32)
        normed = (
            whole
            * lax.rsqrt(jnp.mean(whole * whole, axis=1, keepdims=True) + 1e-06)
            * norm_gain[layer]
        ).astype(jnp.bfloat16)
        value_whole, gate_whole = (
            lax.all_gather(w_value[layer], "sp", axis=0, tiled=True),
            lax.all_gather(w_gate[layer], "sp", axis=0, tiled=True),
        )
        value = jnp.dot(normed, value_whole, preferred_element_type=jnp.float32)
        gate = jnp.dot(normed, gate_whole, preferred_element_type=jnp.float32)
        glu = (value * jax.nn.sigmoid(gate)).astype(jnp.bfloat16)
        before = from_behind(glu[tokens_here - taps :], "sp", 1)
        padded = jnp.concatenate([before[1:], glu], axis=0).astype(jnp.float32)
        conv = lax.conv_general_dilated(
            padded[None],
            conv_taps[layer][:, None, :],
            (1,),
            "VALID",
            dimension_numbers=("NWC", "WIO", "NWC"),
            feature_group_count=local_ch,
            precision=lax.Precision.HIGHEST,
        )[0]
        mean = lax.psum(jnp.sum(conv, axis=1, keepdims=True), "tp") / C
        centred = conv - mean
        spread = lax.psum(jnp.sum(centred * centred, axis=1, keepdims=True), "tp") / C
        act = jax.nn.silu(centred * lax.rsqrt(spread + 1e-05) * channel_gain[layer]).astype(
            jnp.bfloat16
        )
        out_whole = lax.all_gather(w_out[layer], "sp", axis=1, tiled=True)
        terms = jnp.dot(act, out_whole, preferred_element_type=jnp.float32)
        branch = lax.psum_scatter(terms, "tp", scatter_dimension=1, tiled=True)
        x = (x.astype(jnp.float32) + branch).astype(jnp.bfloat16)
    return x


def solution(mesh):
    return jax.shard_map(
        shards,
        mesh=mesh,
        in_specs=(
            P("sp", "tp"),
            P(),
            P(None, "sp", "tp"),
            P(None, "sp", "tp"),
            P(None, None, "tp"),
            P(None, "tp"),
            P(None, "tp", "sp"),
        ),
        out_specs=P("sp", "tp"),
        check_vma=False,
    )
```

profile of v0, /device:TPU:0, one launch (start us, length us, event | category | flops | bytes accessed | tf_op | source)
XLA Modules:
  0.0 370.0 jit_solution(6867189528916284857)
XLA Ops:
  6.5 0.0 copy-start.5
  6.5 0.0 all-gather.15.cloned.1.call-start
  6.5 0.7 all-gather.15.cloned.1.call-update
  7.3 0.0 all-gather.19.cloned.1.call-start
  7.3 1.7 fusion.46
  9.0 0.0 all-gather.19.cloned.1.call-update
  9.0 0.0 all-gather.21.cloned.1.call-start
  9.1 1.7 fusion.45
  10.8 0.0 all-gather.21.cloned.1.call-update
  10.8 0.0 all-gather.23.cloned.1.call-start
  10.8 1.7 fusion.47
  12.5 0.0 all-gather.23.cloned.1.call-update
  12.6 0.0 reduce-scatter.3.cloned.1.call-start
  12.6 0.0 copy-done.5
  12.6 0.0 copy-done.4
  12.7 15.7 %all-gather.15.cloned.1.call-done = bf16[256,2048]{1,0:T(8,128)(2,1)} async-done(((bf16[256,512]{1,0:T(8,128)(2,1)}), bf16[256,2048]{1,0:T(8,128)(2,1)}) %all-gather.15.cloned.1.call-update) | async-done | bytes 1048592 | tf_op jit(solution)/shard_map/all_gather | solution.py:22
  28.4 1.6 fusion
  30.0 40.8 %all-gather.19.cloned.1.call-done = bf16[1,2048,256]{2,1,0:T(8,128)(2,1)} async-done(((bf16[1,256,256]{2,1,0:T(8,128)(2,1)}), bf16[1,2048,256]{2,1,0:T(8,128)(2,1)}) %all-gather.19.cloned.1.call-update) | async-done | bytes 1048592 | tf_op jit(solution)/shard_map/all_gather | solution.py:29
  70.8 2.0 fusion.24
  72.8 0.0 copy-start.6
  72.8 39.1 %all-gather.21.cloned.1.call-done = bf16[1,2048,256]{2,1,0:T(8,128)(2,1)} async-done(((bf16[1,256,256]{2,1,0:T(8,128)(2,1)}), bf16[1,2048,256]{2,1,0:T(8,128)(2,1)}) %all-gather.21.cloned.1.call-update) | async-done | bytes 1048592 | tf_op jit(solution)/shard_map/all_gather | solution.py:30
  111.9 0.0 copy-done.1
  111.9 1.7 fusion.14
  113.7 2.5 collective-permute-start
  116.2 0.0 copy-done.6
  116.2 1.9 collective-permute-done
  118.1 4.8 %fusion.50 = (f32[256]{0:T(256)S(1)}, f32[1,256,256]{2,0,1:T(1,128)S(1)}) fusion(f32[1,128,256]{2,1,0:T(8,128)S(1)} %get-tuple-element.6, bf16[1,383,256]{2,1,0:T(8,128)(2,1)S(1)} %maximum_bitcast_fusion), kind=kOutput, calls=%fused_computation.70 | convolution fusion | flops 100728576 | bytes 590336 | tf_op jit(solution)/shard_map/conv_general_dilated | solution.py:37
  123.0 5.7 %psum.28 = f32[256,1]{0,1:T(1,128)S(1)} all-reduce(f32[256,1]{0,1:T(1,128)S(1)} %bitcast.72), channel_id=1, replica_groups=mesh['sp'=8,'tp'=4] {'tp'}, use_global_device_ids=true, to_apply=%region_2.0 | all-reduce | flops 256 | bytes 2048 | tf_op jit(solution)/shard_map/psum | solution.py:46
  128.6 0.2 multiply_reduce_fusion.1
  128.8 7.0 %psum.29 = f32[256,1]{0,1:T(1,128)S(1)} all-reduce(f32[256,1]{0,1:T(1,128)S(1)} %bitcast.68), channel_id=1, replica_groups=mesh['sp'=8,'tp'=4] {'tp'}, use_global_device_ids=true, to_apply=%region_4.0 | all-reduce | flops 256 | bytes 2048 | tf_op jit(solution)/shard_map/psum | solution.py:48
  135.8 16.2 %all-gather.23.cloned.1.call-done = bf16[1,256,2048]{2,1,0:T(8,128)(2,1)} async-done(((bf16[1,256,256]{2,1,0:T(8,128)(2,1)}), bf16[1,256,2048]{2,1,0:T(8,128)(2,1)}) %all-gather.23.cloned.1.call-update) | async-done | bytes 1048592 | tf_op jit(solution)/shard_map/all_gather | solution.py:52
  152.0 3.1 fusion.21
  155.1 0.0 reduce-scatter.3.cloned.1.call-update
  155.1 0.0 all-gather.17.cloned.1.call-start
  155.2 30.3 %reduce-scatter.3.cloned.1.call-done = f32[256,512]{1,0:T(8,128)} async-done(((f32[256,2048]{1,0:T(8,128)}), f32[256,512]{1,0:T(8,128)}) %reduce-scatter.3.cloned.1.call-update) | async-done | bytes 524304 | tf_op jit(solution)/shard_map/reduce_scatter | solution.py:54
  185.4 0.0 copy-done.3
  185.4 1.8 add_convert_fusion.1
  187.3 0.0 all-gather.17.cloned.1.call-update
  187.3 0.0 all-gather.25.cloned.1.call-start
  187.3 0.7 all-gather.25.cloned.1.call-update
  188.0 0.0 all-gather.27.cloned.1.call-start
  188.1 0.7 all-gather.27.cloned.1.call-update
  188.8 0.0 all-gather.29.cloned.1.call-start
  188.8 0.7 all-gather.29.cloned.1.call-update
  189.5 0.0 reduce-scatter.5.cloned.1.call-start
  189.6 14.6 %all-gather.17.cloned.1.call-done = bf16[256,2048]{1,0:T(8,128)(2,1)} async-done(((bf16[256,512]{1,0:T(8,128)(2,1)}), bf16[256,2048]{1,0:T(8,128)(2,1)}) %all-gather.17.cloned.1.call-update) | async-done | bytes 1048592 | tf_op jit(solution)/shard_map/all_gather | solution.py:22
  204.1 1.6 fusion.3
  205.8 40.8 %all-gather.25.cloned.1.call-done = bf16[1,2048,256]{2,1,0:T(8,128)(2,1)} async-done(((bf16[1,256,256]{2,1,0:T(8,128)(2,1)}), bf16[1,2048,256]{2,1,0:T(8,128)(2,1)}) %all-gather.25.cloned.1.call-update) | async-done | bytes 1048592 | tf_op jit(solution)/shard_map/all_gather | solution.py:29
  246.6 2.0 fusion.19
  248.6 39.1 %all-gather.27.cloned.1.call-done = bf16[1,2048,256]{2,1,0:T(8,128)(2,1)} async-done(((bf16[1,256,256]{2,1,0:T(8,128)(2,1)}), bf16[1,2048,256]{2,1,0:T(8,128)(2,1)}) %all-gather.27.cloned.1.call-update) | async-done | bytes 1048592 | tf_op jit(solution)/shard_map/all_gather | solution.py:30
  287.7 0.0 copy-done.2
  287.7 1.7 fusion.15
  289.5 2.5 collective-permute-start.1
  292.0 1.9 collective-permute-done.1
  293.9 4.8 %fusion.51 = (f32[256]{0:T(256)S(1)}, f32[1,256,256]{2,0,1:T(1,128)S(1)}) fusion(f32[1,128,256]{2,1,0:T(8,128)S(1)} %get-tuple-element.5, bf16[1,383,256]{2,1,0:T(8,128)(2,1)S(1)} %maximum_bitcast_fusion.1), kind=kOutput, calls=%fused_computation.71 | convolution fusion | flops 100728576 | bytes 590336 | tf_op jit(solution)/shard_map/conv_general_dilated | solution.py:37
  298.8 5.7 %psum.30 = f32[256,1]{0,1:T(1,128)S(1)} all-reduce(f32[256,1]{0,1:T(1,128)S(1)} %bitcast.73), channel_id=1, replica_groups=mesh['sp'=8,'tp'=4] {'tp'}, use_global_device_ids=true, to_apply=%region_8.9 | all-reduce | flops 256 | bytes 2048 | tf_op jit(solution)/shard_map/psum | solution.py:46
  304.4 0.2 multiply_reduce_fusion
  304.6 7.0 %psum.31 = f32[256,1]{0,1:T(1,128)S(1)} all-reduce(f32[256,1]{0,1:T(1,128)S(1)} %bitcast.69), channel_id=1, replica_groups=mesh['sp'=8,'tp'=4] {'tp'}, use_global_device_ids=true, to_apply=%region_10.11 | all-reduce | flops 256 | bytes 2048 | tf_op jit(solution)/shard_map/psum | solution.py:48
  311.6 16.3 %all-gather.29.cloned.1.call-done = bf16[1,256,2048]{2,1,0:T(8,128)(2,1)} async-done(((bf16[1,256,256]{2,1,0:T(8,128)(2,1)}), bf16[1,256,2048]{2,1,0:T(8,128)(2,1)}) %all-gather.29.cloned.1.call-update) | async-done | bytes 1048592 | tf_op jit(solution)/shard_map/all_gather | solution.py:52
  327.9 3.1 fusion.16
  331.0 0.0 reduce-scatter.5.cloned.1.call-update
  331.1 30.3 %reduce-scatter.5.cloned.1.call-done = f32[256,512]{1,0:T(8,128)} async-done(((f32[256,2048]{1,0:T(8,128)}), f32[256,512]{1,0:T(8,128)}) %reduce-scatter.5.cloned.1.call-update) | async-done | bytes 524304 | tf_op jit(solution)/shard_map/reduce_scatter | solution.py:54
  361.4 0.0 copy-done
  361.4 1.8 add_convert_fusion
  (20 shorter events, 0.2 us)
Async XLA Ops:
  6.5 6.1 %copy-start.5 = (f32[2,2048]{1,0:T(2,128)S(1)}, f32[2,2048]{1,0:T(2,128)}, u32[]{:S(2)}) copy-start(f32[2,2048]{1,0:T(2,128)} %param.8) | copy-start | bytes 49156
  6.5 6.1 %copy-start.4 = (f32[2,128,256]{2,1,0:T(8,128)S(1)}, f32[2,128,256]{2,1,0:T(8,128)}, u32[]{:S(2)}) copy-start(f32[2,128,256]{2,1,0:T(8,128)} %param.11) | copy-start | bytes 786436
  6.5 21.8 %all-gather.15.cloned.1.call-start = ((), (), s32[]{:S(2)}) async-start(), calls=%async_computation.2 | async-start | bytes 1310720 | tf_op jit(solution)/shard_map/all_gather | solution.py:22
  7.3 63.5 %all-gather.19.cloned.1.call-start = ((), (), s32[]{:S(2)}) async-start(), calls=%async_computation.6 | async-start | bytes 1179648 | tf_op jit(solution)/shard_map/all_gather | solution.py:29
  9.0 102.9 %all-gather.21.cloned.1.call-start = ((), (), s32[]{:S(2)}) async-start(), calls=%async_computation.7 | async-start | bytes 1179648 | tf_op jit(solution)/shard_map/all_gather | solution.py:30
  10.8 141.2 %all-gather.23.cloned.1.call-start = ((), (), s32[]{:S(2)}) async-start(), calls=%async_computation.8 | async-start | bytes 1179648 | tf_op jit(solution)/shard_map/all_gather | solution.py:52
  12.6 172.9 %reduce-scatter.3.cloned.1.call-start = ((), (), s32[]{:S(2)}) async-start(), calls=%async_computation.3 | async-start | bytes 2621440 | tf_op jit(solution)/shard_map/reduce_scatter | solution.py:54
  28.4 83.6 %copy-start.1 = (bf16[256,2048]{1,0:T(8,128)(2,1)S(1)}, bf16[256,2048]{1,0:T(8,128)(2,1)}, u32[]{:S(2)}) copy-start(bf16[256,2048]{1,0:T(8,128)(2,1)} %all-gather.15.cloned.1.call-done) | copy-start | bytes 3145732
  72.8 43.4 %copy-start.6 = (f32[2,256]{1,0:T(2,128)S(1)}, f32[2,256]{1,0:T(2,128)}, u32[]{:S(2)}) copy-start(f32[2,256]{1,0:T(2,128)} %param.12) | copy-start | bytes 6148
  113.7 4.4 %collective-permute-start = (bf16[128,256]{1,0:T(8,128)(2,1)S(1)}, bf16[128,256]{1,0:T(8,128)(2,1)S(1)}, u32[]{:S(2)}, u32[]{:S(2)}) collective-permute-start(bf16[128,256]{1,0:T(8,128)(2,1)S(1)} %slice.64), channel_id=1, source_target_pairs={{0,4},{4,8},{8,12},{12,16},{16,20},{20,24},{24,28},{1,5},{5,9},{9,... | collective-permute-start | bytes 196616 | tf_op jit(solution)/shard_map/ppermute | solution.py:13
  152.0 33.5 %copy-start.3 = (bf16[256,512]{1,0:T(8,128)(2,1)S(1)}, bf16[256,512]{1,0:T(8,128)(2,1)}, u32[]{:S(2)}) copy-start(bf16[256,512]{1,0:T(8,128)(2,1)} %param.7) | copy-start | bytes 786436
  155.1 49.0 %all-gather.17.cloned.1.call-start = ((), (), s32[]{:S(2)}) async-start(), calls=%async_computation.4 | async-start | bytes 1310720 | tf_op jit(solution)/shard_map/all_gather | solution.py:22
  187.3 59.3 %all-gather.25.cloned.1.call-start = ((), (), s32[]{:S(2)}) async-start(), calls=%async_computation.9 | async-start | bytes 1179648 | tf_op jit(solution)/shard_map/all_gather | solution.py:29
  188.0 99.7 %all-gather.27.cloned.1.call-start = ((), (), s32[]{:S(2)}) async-start(), calls=%async_computation.10 | async-start | bytes 1179648 | tf_op jit(solution)/shard_map/all_gather | solution.py:30
  188.8 139.1 %all-gather.29.cloned.1.call-start = ((), (), s32[]{:S(2)}) async-start(), calls=%async_computation.11 | async-start | bytes 1179648 | tf_op jit(solution)/shard_map/all_gather | solution.py:52
  189.5 171.9 %reduce-scatter.5.cloned.1.call-start = ((), (), s32[]{:S(2)}) async-start(), calls=%async_computation.5 | async-start | bytes 2621440 | tf_op jit(solution)/shard_map/reduce_scatter | solution.py:54
  204.1 83.6 %copy-start.2 = (bf16[256,2048]{1,0:T(8,128)(2,1)S(1)}, bf16[256,2048]{1,0:T(8,128)(2,1)}, u32[]{:S(2)}) copy-start(bf16[256,2048]{1,0:T(8,128)(2,1)} %all-gather.17.cloned.1.call-done) | copy-start | bytes 3145732
  289.5 4.4 %collective-permute-start.1 = (bf16[128,256]{1,0:T(8,128)(2,1)S(1)}, bf16[128,256]{1,0:T(8,128)(2,1)S(1)}, u32[]{:S(2)}, u32[]{:S(2)}) collective-permute-start(bf16[128,256]{1,0:T(8,128)(2,1)S(1)} %slice.66), channel_id=1, source_target_pairs={{0,4},{4,8},{8,12},{12,16},{16,20},{20,24},{24,28},{1,5},{5,9},{9,... | collective-permute-start | bytes 196616 | tf_op jit(solution)/shard_map/ppermute | solution.py:13
  327.9 33.5 %copy-start = (bf16[256,512]{1,0:T(8,128)(2,1)S(1)}, bf16[256,512]{1,0:T(8,128)(2,1)}, u32[]{:S(2)}) copy-start(bf16[256,512]{1,0:T(8,128)(2,1)} %add_convert_fusion.1) | copy-start | bytes 786436
Sparse Core Ops, SparseCore 0:
  8.9 19.4 all-gather.14
  30.5 40.2 all-gather.18
  72.9 38.9 all-gather.20
  113.8 38.0 all-gather.22
  155.2 30.1 reduce-scatter.2
  187.4 16.6 all-gather.16
  206.3 40.2 all-gather.24
  248.7 38.9 all-gather.26
  289.8 38.0 all-gather.28
  331.2 30.1 reduce-scatter.4
where the time goes:
time: 371 us; the launch traced here: 370 us
  waiting for transfers between devices  290 us (78%)
  blocking collectives  25.3 us (7%)
  matrix products  23.4 us (6%)
  between operations  13.7 us (4%)
  other arithmetic  7.31 us (2%)
  starting transfers between devices  5.32 us (1%)
  local copies, waits for them, and re-layouts  5.19 us (1%)
    all_gather x2, waiting for transfers between devices, shards(): lax.all_gather(w_value[layer], 'sp', axis=0, tiled=True)  81.7 us
    all_gather x2, waiting for transfers between devices, shards(): lax.all_gather(w_gate[layer], 'sp', axis=0, tiled=True)  78.2 us
    reduce_scatter x2, waiting for transfers between devices, shards(): branch = lax.psum_scatter(terms, 'tp', scatter_dimension=1, tiled=True)  60.6 us
    all_gather x2, waiting for transfers between devices, shards(): out_whole = lax.all_gather(w_out[layer], 'sp', axis=1, tiled=True)  32.5 us
    all_gather x2, waiting for transfers between devices, shards(): whole = lax.all_gather(x, 'tp', axis=1, tiled=True).astype(jnp.float32)  30.3 us
    psum x2, blocking collectives, shards(): lax.psum(jnp.sum(centred * centred, axis=1, keepdims=True), 'tp') / C  14 us
    psum x2, blocking collectives, shards(): mean = lax.psum(jnp.sum(conv, axis=1, keepdims=True), 'tp') / C  11.3 us
    conv_general_dilated x2, matrix products, shards(): lax.conv_general_dilated(padded[None], conv_taps[layer][:, None, :], (1,)...  9.67 us
  transfers between devices with their start and end apart: 12, of which 12 were waited for; matrix products, arithmetic and copies ran while one was open for 7% of the time, Pallas kernels for 0%

commit v1 on v0

--- a/solution.py
+++ b/solution.py
@@ -49,7 +49,7 @@
         act = jax.nn.silu(centred * lax.rsqrt(spread + 1e-05) * channel_gain[layer]).astype(
             jnp.bfloat16
         )
-        out_whole = lax.all_gather(w_out[layer], "sp", axis=1, tiled=True)
+        out_whole = jnp.concatenate(lax.all_gather(w_out[layer], "sp"), axis=1)
         terms = jnp.dot(act, out_whole, preferred_element_type=jnp.float32)
         branch = lax.psum_scatter(terms, "tp", scatter_dimension=1, tiled=True)
         x = (x.astype(jnp.float32) + branch).astype(jnp.bfloat16)

time: 371 us -> 406 us (1.094)
  waiting for transfers between devices: 290 us -> 326 us
    all_gather x2, waiting for transfers between devices: 32.5 us -> 73.6 us  [shards(): out_whole = jnp.concatenate(lax.all_gather(w_out[layer], 'sp'), axis=1)]
  transfers between devices with their start and end apart: 12 -> 12, of which waited for: 12 -> 10; matrix products, arithmetic and copies ran while one was open for 7% -> 5% of each run, Pallas kernels for 0% -> 0%
where the time goes in v1:
time: 406 us; the launch traced here: 405 us
  waiting for transfers between devices  326 us (80%)
  blocking collectives  24.5 us (6%)
  matrix products  20.9 us (5%)
  between operations  13.7 us (3%)
  local copies, waits for them, and re-layouts  8.14 us (2%)
  other arithmetic  7.31 us (2%)
  starting transfers between devices  5.32 us (1%)
    all_gather x2, waiting for transfers between devices, shards(): lax.all_gather(w_value[layer], 'sp', axis=0, tiled=True)  81.7 us
    all_gather x2, waiting for transfers between devices, shards(): lax.all_gather(w_gate[layer], 'sp', axis=0, tiled=True)  78.2 us
    all_gather x2, waiting for transfers between devices, shards(): out_whole = jnp.concatenate(lax.all_gather(w_out[layer], 'sp'), axis=1)  73.6 us
    reduce_scatter x2, waiting for transfers between devices, shards(): branch = lax.psum_scatter(terms, 'tp', scatter_dimension=1, tiled=True)  58.9 us
    all_gather x2, waiting for transfers between devices, shards(): whole = lax.all_gather(x, 'tp', axis=1, tiled=True).astype(jnp.float32)  30.2 us
    psum x2, blocking collectives, shards(): lax.psum(jnp.sum(centred * centred, axis=1, keepdims=True), 'tp') / C  13.2 us
    psum x2, blocking collectives, shards(): mean = lax.psum(jnp.sum(conv, axis=1, keepdims=True), 'tp') / C  11.3 us
    conv_general_dilated x2, matrix products, shards(): lax.conv_general_dilated(padded[None], conv_taps[layer][:, None, :], (1,)...  9.67 us
  transfers between devices with their start and end apart: 12, of which 10 were waited for; matrix products, arithmetic and copies ran while one was open for 5% of the time, Pallas kernels for 0%

profile of v1, /device:TPU:0, one launch (start us, length us, event | category | flops | bytes accessed | tf_op | source)
XLA Modules:
  0.0 405.4 jit_solution(7602448940463626116)
XLA Ops:
  6.5 0.0 all-gather.13.cloned.1.call-start
  6.5 0.7 all-gather.13.cloned.1.call-update
  7.3 0.0 all-gather.21.cloned.1.call-start
  7.3 1.7 fusion.48
  9.0 0.0 all-gather.21.cloned.1.call-update
  9.0 0.0 all-gather.23.cloned.1.call-start
  9.1 1.7 fusion.47
  10.8 0.0 all-gather.23.cloned.1.call-update
  10.8 0.0 all-gather.15.cloned.1.call-start
  10.8 1.7 fusion.49
  12.5 0.0 all-gather.15.cloned.1.call-update
  12.6 0.0 reduce-scatter.3.cloned.1.call-start
  12.6 0.0 copy-done.4
  12.6 0.0 copy-done.5
  12.7 15.7 %all-gather.13.cloned.1.call-done = bf16[256,2048]{1,0:T(8,128)(2,1)} async-done(((bf16[256,512]{1,0:T(8,128)(2,1)}), bf16[256,2048]{1,0:T(8,128)(2,1)}) %all-gather.13.cloned.1.call-update) | async-done | bytes 1048592 | tf_op jit(solution)/shard_map/all_gather | solution.py:22
  28.4 1.6 fusion
  30.0 40.8 %all-gather.21.cloned.1.call-done = bf16[1,2048,256]{2,1,0:T(8,128)(2,1)} async-done(((bf16[1,256,256]{2,1,0:T(8,128)(2,1)}), bf16[1,2048,256]{2,1,0:T(8,128)(2,1)}) %all-gather.21.cloned.1.call-update) | async-done | bytes 1048592 | tf_op jit(solution)/shard_map/all_gather | solution.py:29
  70.8 2.0 fusion.20
  72.8 0.0 copy-start.6
  72.8 39.1 %all-gather.23.cloned.1.call-done = bf16[1,2048,256]{2,1,0:T(8,128)(2,1)} async-done(((bf16[1,256,256]{2,1,0:T(8,128)(2,1)}), bf16[1,2048,256]{2,1,0:T(8,128)(2,1)}) %all-gather.23.cloned.1.call-update) | async-done | bytes 1048592 | tf_op jit(solution)/shard_map/all_gather | solution.py:30
  111.9 0.0 copy-done.1
  111.9 1.7 fusion.14
  113.7 2.5 collective-permute-start
  116.2 0.0 copy-done.6
  116.2 36.7 %all-gather.15.cloned.1.call-done = bf16[8,256,256]{2,1,0:T(8,128)(2,1)} async-done(((bf16[1,256,256]{2,1,0:T(8,128)(2,1)}), bf16[8,256,256]{2,1,0:T(8,128)(2,1)}) %all-gather.15.cloned.1.call-update) | async-done | bytes 1048592 | tf_op jit(solution)/shard_map/all_gather | solution.py:52
  152.9 1.5 copy.27
  154.4 0.0 collective-permute-done
  154.5 4.8 %fusion.52 = (f32[256]{0:T(256)S(1)}, f32[1,256,256]{2,0,1:T(1,128)S(1)}) fusion(f32[1,128,256]{2,1,0:T(8,128)S(1)} %get-tuple-element.6, bf16[1,383,256]{2,1,0:T(8,128)(2,1)S(1)} %maximum_bitcast_fusion), kind=kOutput, calls=%fused_computation.70 | convolution fusion | flops 100728576 | bytes 590336 | tf_op jit(solution)/shard_map/conv_general_dilated | solution.py:37
  159.3 5.7 %psum.28 = f32[256,1]{0,1:T(1,128)S(1)} all-reduce(f32[256,1]{0,1:T(1,128)S(1)} %bitcast.80), channel_id=1, replica_groups=mesh['sp'=8,'tp'=4] {'tp'}, use_global_device_ids=true, to_apply=%region_2.0 | all-reduce | flops 256 | bytes 2048 | tf_op jit(solution)/shard_map/psum | solution.py:46
  165.0 0.2 fusion.33
  165.2 6.6 %psum.29 = f32[256,1]{0,1:T(1,128)S(1)} all-reduce(f32[256,1]{0,1:T(1,128)S(1)} %bitcast.76), channel_id=1, replica_groups=mesh['sp'=8,'tp'=4] {'tp'}, use_global_device_ids=true, to_apply=%region_4.0 | all-reduce | flops 256 | bytes 2048 | tf_op jit(solution)/shard_map/psum | solution.py:48
  171.8 1.8 fusion.36
  173.7 0.0 reduce-scatter.3.cloned.1.call-update
  173.7 0.0 all-gather.17.cloned.1.call-start
  173.7 29.4 %reduce-scatter.3.cloned.1.call-done = f32[256,512]{1,0:T(8,128)} async-done(((f32[256,2048]{1,0:T(8,128)}), f32[256,512]{1,0:T(8,128)}) %reduce-scatter.3.cloned.1.call-update) | async-done | bytes 524304 | tf_op jit(solution)/shard_map/reduce_scatter | solution.py:54
  203.1 0.0 copy-done.3
  203.1 1.8 add_convert_fusion.1
  204.9 0.0 all-gather.17.cloned.1.call-update
  205.0 0.0 all-gather.25.cloned.1.call-start
  205.0 0.7 all-gather.25.cloned.1.call-update
  205.7 0.0 all-gather.27.cloned.1.call-start
  205.8 0.7 all-gather.27.cloned.1.call-update
  206.5 0.0 all-gather.19.cloned.1.call-start
  206.5 0.7 all-gather.19.cloned.1.call-update
  207.2 0.0 reduce-scatter.5.cloned.1.call-start
  207.3 14.6 %all-gather.17.cloned.1.call-done = bf16[256,2048]{1,0:T(8,128)(2,1)} async-done(((bf16[256,512]{1,0:T(8,128)(2,1)}), bf16[256,2048]{1,0:T(8,128)(2,1)}) %all-gather.17.cloned.1.call-update) | async-done | bytes 1048592 | tf_op jit(solution)/shard_map/all_gather | solution.py:22
  221.8 1.6 fusion.3
  223.4 40.8 %all-gather.25.cloned.1.call-done = bf16[1,2048,256]{2,1,0:T(8,128)(2,1)} async-done(((bf16[1,256,256]{2,1,0:T(8,128)(2,1)}), bf16[1,2048,256]{2,1,0:T(8,128)(2,1)}) %all-gather.25.cloned.1.call-update) | async-done | bytes 1048592 | tf_op jit(solution)/shard_map/all_gather | solution.py:29
  264.3 2.0 fusion.17
  266.3 39.1 %all-gather.27.cloned.1.call-done = bf16[1,2048,256]{2,1,0:T(8,128)(2,1)} async-done(((bf16[1,256,256]{2,1,0:T(8,128)(2,1)}), bf16[1,2048,256]{2,1,0:T(8,128)(2,1)}) %all-gather.27.cloned.1.call-update) | async-done | bytes 1048592 | tf_op jit(solution)/shard_map/all_gather | solution.py:30
  305.4 1.7 fusion.15
  307.2 2.5 collective-permute-start.1
  309.6 36.9 %all-gather.19.cloned.1.call-done = bf16[8,256,256]{2,1,0:T(8,128)(2,1)} async-done(((bf16[1,256,256]{2,1,0:T(8,128)(2,1)}), bf16[8,256,256]{2,1,0:T(8,128)(2,1)}) %all-gather.19.cloned.1.call-update) | async-done | bytes 1048592 | tf_op jit(solution)/shard_map/all_gather | solution.py:52
  346.6 1.5 copy.31
  348.0 0.0 collective-permute-done.1
  348.1 4.8 %fusion.53 = (f32[256]{0:T(256)S(1)}, f32[1,256,256]{2,0,1:T(1,128)S(1)}) fusion(f32[1,128,256]{2,1,0:T(8,128)S(1)} %get-tuple-element.5, bf16[1,383,256]{2,1,0:T(8,128)(2,1)S(1)} %maximum_bitcast_fusion.1), kind=kOutput, calls=%fused_computation.71 | convolution fusion | flops 100728576 | bytes 590336 | tf_op jit(solution)/shard_map/conv_general_dilated | solution.py:37
  353.0 5.7 %psum.30 = f32[256,1]{0,1:T(1,128)S(1)} all-reduce(f32[256,1]{0,1:T(1,128)S(1)} %bitcast.81), channel_id=1, replica_groups=mesh['sp'=8,'tp'=4] {'tp'}, use_global_device_ids=true, to_apply=%region_8.9 | all-reduce | flops 256 | bytes 2048 | tf_op jit(solution)/shard_map/psum | solution.py:46
  358.6 0.2 fusion.31
  358.8 6.6 %psum.31 = f32[256,1]{0,1:T(1,128)S(1)} all-reduce(f32[256,1]{0,1:T(1,128)S(1)} %bitcast.77), channel_id=1, replica_groups=mesh['sp'=8,'tp'=4] {'tp'}, use_global_device_ids=true, to_apply=%region_10.11 | all-reduce | flops 256 | bytes 2048 | tf_op jit(solution)/shard_map/psum | solution.py:48
  365.4 1.8 fusion.34
  367.3 0.0 reduce-scatter.5.cloned.1.call-update
  367.3 29.5 %reduce-scatter.5.cloned.1.call-done = f32[256,512]{1,0:T(8,128)} async-done(((f32[256,2048]{1,0:T(8,128)}), f32[256,512]{1,0:T(8,128)}) %reduce-scatter.5.cloned.1.call-update) | async-done | bytes 524304 | tf_op jit(solution)/shard_map/reduce_scatter | solution.py:54
  396.8 0.0 copy-done
  396.8 1.8 add_convert_fusion
  (22 shorter events, 0.2 us)
Async XLA Ops:
  6.5 6.1 %copy-start.4 = (f32[2,128,256]{2,1,0:T(8,128)S(1)}, f32[2,128,256]{2,1,0:T(8,128)}, u32[]{:S(2)}) copy-start(f32[2,128,256]{2,1,0:T(8,128)} %param.11) | copy-start | bytes 786436
  6.5 6.1 %copy-start.5 = (f32[2,2048]{1,0:T(2,128)S(1)}, f32[2,2048]{1,0:T(2,128)}, u32[]{:S(2)}) copy-start(f32[2,2048]{1,0:T(2,128)} %param.8) | copy-start | bytes 49156
  6.5 21.8 %all-gather.13.cloned.1.call-start = ((), (), s32[]{:S(2)}) async-start(), calls=%async_computation.2 | async-start | bytes 1310720 | tf_op jit(solution)/shard_map/all_gather | solution.py:22
  7.3 63.5 %all-gather.21.cloned.1.call-start = ((), (), s32[]{:S(2)}) async-start(), calls=%async_computation.8 | async-start | bytes 1179648 | tf_op jit(solution)/shard_map/all_gather | solution.py:29
  9.0 102.9 %all-gather.23.cloned.1.call-start = ((), (), s32[]{:S(2)}) async-start(), calls=%async_computation.9 | async-start | bytes 1179648 | tf_op jit(solution)/shard_map/all_gather | solution.py:30
  10.8 142.1 %all-gather.15.cloned.1.call-start = ((), (), s32[]{:S(2)}) async-start(), calls=%async_computation.3 | async-start | bytes 1179648 | tf_op jit(solution)/shard_map/all_gather | solution.py:52
  12.6 190.6 %reduce-scatter.3.cloned.1.call-start = ((), (), s32[]{:S(2)}) async-start(), calls=%async_computation.4 | async-start | bytes 2621440 | tf_op jit(solution)/shard_map/reduce_scatter | solution.py:54
  28.4 83.6 %copy-start.1 = (bf16[256,2048]{1,0:T(8,128)(2,1)S(1)}, bf16[256,2048]{1,0:T(8,128)(2,1)}, u32[]{:S(2)}) copy-start(bf16[256,2048]{1,0:T(8,128)(2,1)} %all-gather.13.cloned.1.call-done) | copy-start | bytes 3145732
  72.8 43.4 %copy-start.6 = (f32[2,256]{1,0:T(2,128)S(1)}, f32[2,256]{1,0:T(2,128)}, u32[]{:S(2)}) copy-start(f32[2,256]{1,0:T(2,128)} %param.12) | copy-start | bytes 6148
  113.7 40.7 %collective-permute-start = (bf16[128,256]{1,0:T(8,128)(2,1)S(1)}, bf16[128,256]{1,0:T(8,128)(2,1)S(1)}, u32[]{:S(2)}, u32[]{:S(2)}) collective-permute-start(bf16[128,256]{1,0:T(8,128)(2,1)S(1)} %slice.64), channel_id=1, source_target_pairs={{0,4},{4,8},{8,12},{12,16},{16,20},{20,24},{24,28},{1,5},{5,9},{9,... | collective-permute-start | bytes 196616 | tf_op jit(solution)/shard_map/ppermute | solution.py:13
  171.8 31.3 %copy-start.3 = (bf16[256,512]{1,0:T(8,128)(2,1)S(1)}, bf16[256,512]{1,0:T(8,128)(2,1)}, u32[]{:S(2)}) copy-start(bf16[256,512]{1,0:T(8,128)(2,1)} %param.7) | copy-start | bytes 786436
  173.7 48.1 %all-gather.17.cloned.1.call-start = ((), (), s32[]{:S(2)}) async-start(), calls=%async_computation.5 | async-start | bytes 1310720 | tf_op jit(solution)/shard_map/all_gather | solution.py:22
  205.0 59.3 %all-gather.25.cloned.1.call-start = ((), (), s32[]{:S(2)}) async-start(), calls=%async_computation.10 | async-start | bytes 1179648 | tf_op jit(solution)/shard_map/all_gather | solution.py:29
  205.7 99.7 %all-gather.27.cloned.1.call-start = ((), (), s32[]{:S(2)}) async-start(), calls=%async_computation.11 | async-start | bytes 1179648 | tf_op jit(solution)/shard_map/all_gather | solution.py:30
  206.5 140.1 %all-gather.19.cloned.1.call-start = ((), (), s32[]{:S(2)}) async-start(), calls=%async_computation.6 | async-start | bytes 1179648 | tf_op jit(solution)/shard_map/all_gather | solution.py:52
  207.2 189.6 %reduce-scatter.5.cloned.1.call-start = ((), (), s32[]{:S(2)}) async-start(), calls=%async_computation.7 | async-start | bytes 2621440 | tf_op jit(solution)/shard_map/reduce_scatter | solution.py:54
  221.8 83.6 %copy-start.2 = (bf16[256,2048]{1,0:T(8,128)(2,1)S(1)}, bf16[256,2048]{1,0:T(8,128)(2,1)}, u32[]{:S(2)}) copy-start(bf16[256,2048]{1,0:T(8,128)(2,1)} %all-gather.17.cloned.1.call-done) | copy-start | bytes 3145732
  307.2 40.9 %collective-permute-start.1 = (bf16[128,256]{1,0:T(8,128)(2,1)S(1)}, bf16[128,256]{1,0:T(8,128)(2,1)S(1)}, u32[]{:S(2)}, u32[]{:S(2)}) collective-permute-start(bf16[128,256]{1,0:T(8,128)(2,1)S(1)} %slice.66), channel_id=1, source_target_pairs={{0,4},{4,8},{8,12},{12,16},{16,20},{20,24},{24,28},{1,5},{5,9},{9,... | collective-permute-start | bytes 196616 | tf_op jit(solution)/shard_map/ppermute | solution.py:13
  365.4 31.4 %copy-start = (bf16[256,512]{1,0:T(8,128)(2,1)S(1)}, bf16[256,512]{1,0:T(8,128)(2,1)}, u32[]{:S(2)}) copy-start(bf16[256,512]{1,0:T(8,128)(2,1)} %add_convert_fusion.1) | copy-start | bytes 786436
Sparse Core Ops, SparseCore 0:
  8.9 19.4 all-gather.12
  30.5 40.2 all-gather.20
  72.9 38.9 all-gather.22
  113.9 38.9 all-gather.14
  173.8 29.2 reduce-scatter.2
  205.1 16.6 all-gather.16
  223.9 40.2 all-gather.24
  266.4 38.9 all-gather.26
  307.5 38.9 all-gather.18
  367.4 29.3 reduce-scatter.4
